TPU v7x, 32 devices: a whole 2x2x4 slice. The times are simulated.
32 devices in a mesh: sp: 8 (over z, x), dp: 4 (over y, core).
Axes of the slice: x: 2, y: 2, z: 4, core: 2. Of those that a mesh axis runs over, the one named last changes fastest.
Arguments:
- skip_stream_entering: bfloat16 [4, 1024, 2048], P('dp', 'sp'), may hold values from -6 to 6
- mapped_probe_matrix: bfloat16 [4, 1024, 2048], P('dp', 'sp'), may hold values from -6 to 6
- mapped_lookup_matrix: bfloat16 [4, 1024, 2048], P('dp', 'sp'), may hold values from -6 to 6
- mapped_content_matrix: bfloat16 [4, 1024, 4096], P('dp', 'sp'), may hold values from -6 to 6
- retention_preactivation: bfloat16 [4, 1024, 2048], P('dp', 'sp'), may hold values from -4 to 12
- extra_shrinkage: float32 [4, 16, 1024], P('dp', 'sp'), may hold values from -0.6932 to 0
- attention_group_scale: float32 [4096], replicated, may hold values from 0.1 to 1.9
- final_projection_matrix: bfloat16 [4096, 2048], P(None, 'dp'), may hold values from -0.09375 to 0.09375
- blender_branch_scale: float32 [2048], replicated, may hold values from 0.1 to 1.9
- specialist_prenormal_scale: float32 [2048], replicated, may hold values from 0.1 to 1.9
- specialist_switch_matrix: bfloat16 [32, 2048, 1024], P(('sp', 'dp')), may hold values from -0.125 to 0.125
- specialist_expand_matrix: bfloat16 [32, 2048, 1024], P(('sp', 'dp')), may hold values from -0.125 to 0.125
- specialist_contract_matrix: bfloat16 [32, 1024, 2048], P(('sp', 'dp')), may hold values from -0.1875 to 0.1875
- specialist_branch_scale: float32 [2048], replicated, may hold values from 0.1 to 1.9
- assigned_specialists: int32 [4, 1024, 2], P('dp', 'sp'), may hold values from 0 to 31, all different within a row; in each aligned block of 128 rows (0 to 127, 128 to 255, ..., all dimensions but the last counted through in order) at most 13 rows name the same one
- dispatcher_logits: float32 [4, 1024, 2], P('dp', 'sp'), may hold values from 0.2 to 1
Outputs:
- layer_out: bfloat16 [4, 1024, 2048], P('dp', 'sp')
Inputs may be any that keep to these rules, and one draw needn't show every extreme that they name: `assigned_specialists`: in the rows of one device no expert is named more than 13 times; in every draw some expert reaches 13 on some device.
All inputs are finite; a program needn't handle non-finite values.
Results may differ from a plain program's by a relative error of at most 0.013.
Values may be sent and summed in bfloat16 or wider, within the bound.
A program may use at most 128 MiB of HBM per device.

v0:
```python
import jax
import jax.numpy as jnp
from jax import lax
from jax.sharding import PartitionSpec as P

D = 2048
ATTENTION_GROUPS = 16
KEY_WIDTH = 128
DV = 256
TOP = 2
BLOCK = 64
epsilon = 1e-06
softness_factor = 16.0
highest = lax.Precision.HIGHEST


def rms_scale(values, gain):
    mean_square = jnp.mean(values * values, axis=-1, keepdims=True)
    return values * lax.rsqrt(mean_square + epsilon) * gain


def combine_states(earlier, later):
    return (earlier[0] * later[0], later[0][..., None] * earlier[1] + later[1])


def block_attention(query_f, key_f, value_f, shrink_exponent):
    length_value, head_count, key_dim = query_f.shape
    value_dim = value_f.shape[-1]
    block_count = length_value // BLOCK
    query_blocks = query_f.reshape(block_count, BLOCK, head_count, key_dim)
    key_blocks = key_f.reshape(block_count, BLOCK, head_count, key_dim)
    value_blocks = value_f.reshape(block_count, BLOCK, head_count, value_dim)
    within = jnp.cumsum(shrink_exponent.reshape(block_count, BLOCK, head_count, key_dim), axis=1)
    block_end = within[:, -1]
    lifted = query_blocks * jnp.exp(within)
    lowered = key_blocks * jnp.exp(-within)
    scores = jnp.einsum("nthk,nshk->nhts", lifted, lowered, precision=highest)
    causal = jnp.arange(BLOCK)[:, None] >= jnp.arange(BLOCK)[None, :]
    scores = jnp.where(causal, scores, 0.0)
    inside = jnp.einsum("nhts,nshv->nthv", scores, value_blocks, precision=highest)
    carried_keys = key_blocks * jnp.exp(block_end[:, None] - within)
    updates = jnp.einsum("nshk,nshv->nhkv", carried_keys, value_blocks, precision=highest)
    decays = jnp.exp(block_end)
    total_decay, states = lax.associative_scan(combine_states, (decays, updates), axis=0)
    entering = jnp.concatenate([jnp.zeros_like(states[:1]), states[:-1]], axis=0)
    across = jnp.einsum("nthk,nhkv->nthv", lifted, entering, precision=highest)
    outputs = (inside + across).reshape(length_value, head_count, value_dim)
    offsets = jnp.cumsum(block_end, axis=0) - block_end
    reached = (query_blocks * jnp.exp(within + offsets[:, None])).reshape(
        length_value, head_count, key_dim
    )
    return (outputs, total_decay[-1], states[-1], reached)


def shards(
    skip_stream_entering,
    mapped_probe_matrix,
    mapped_lookup_matrix,
    mapped_content_matrix,
    retention_preactivation,
    extra_shrinkage,
    attention_group_scale,
    final_projection_matrix,
    blender_branch_scale,
    specialist_prenormal_scale,
    specialist_switch_matrix,
    specialist_expand_matrix,
    specialist_contract_matrix,
    specialist_branch_scale,
    assigned_specialists,
    dispatcher_logits,
):
    tok_rows = mapped_probe_matrix.shape[1]
    sp_count = lax.axis_size("sp")
    dp_count = lax.axis_size("dp")
    query_local = mapped_probe_matrix[0].reshape(tok_rows, ATTENTION_GROUPS, KEY_WIDTH)
    key_local = mapped_lookup_matrix[0].reshape(tok_rows, ATTENTION_GROUPS, KEY_WIDTH)
    value_local = mapped_content_matrix[0].reshape(tok_rows, ATTENTION_GROUPS, DV)
    decay_local = retention_preactivation[0].reshape(tok_rows, ATTENTION_GROUPS, KEY_WIDTH)
    arrived = (
        lax.all_to_all(query_local, "sp", split_axis=1, concat_axis=0, tiled=True),
        lax.all_to_all(key_local, "sp", split_axis=1, concat_axis=0, tiled=True),
        lax.all_to_all(value_local, "sp", split_axis=1, concat_axis=0, tiled=True),
        lax.all_to_all(decay_local, "sp", split_axis=1, concat_axis=0, tiled=True),
    )
    query_head, key_head, value_head, head_decay = arrived
    own_heads = query_head.shape[1]
    shrink_exponent = jax.nn.log_sigmoid(head_decay.astype(jnp.float32)) / softness_factor
    shrink_exponent = shrink_exponent + jnp.transpose(extra_shrinkage[0])[:, :, None]
    outputs = block_attention(
        query_head.astype(jnp.float32) * KEY_WIDTH ** (-0.5),
        key_head.astype(jnp.float32),
        value_head.astype(jnp.float32),
        shrink_exponent,
    )[0]
    offset = lax.axis_index("sp") * (own_heads * DV)
    gains = lax.dynamic_slice_in_dim(attention_group_scale, offset, own_heads * DV).reshape(
        own_heads, DV
    )
    normed = rms_scale(outputs, gains).astype(jnp.bfloat16)
    attention_group_result = lax.all_to_all(normed, "sp", split_axis=0, concat_axis=1, tiled=True)
    flat_heads = attention_group_result.reshape(tok_rows, ATTENTION_GROUPS * DV)
    projected = jnp.dot(
        flat_heads,
        lax.all_gather(final_projection_matrix, "dp", axis=1, tiled=True),
        preferred_element_type=jnp.float32,
    ).astype(jnp.bfloat16)
    stream = skip_stream_entering[0].astype(jnp.float32)
    residual = (stream + rms_scale(projected.astype(jnp.float32), blender_branch_scale)).astype(
        jnp.bfloat16
    )
    expert_in = rms_scale(residual.astype(jnp.float32), specialist_prenormal_scale).astype(
        jnp.bfloat16
    )
    expert_total = sp_count * dp_count
    capacity = max(2, 5 * tok_rows * TOP // (3 * expert_total))
    chosen = assigned_specialists[0].reshape(-1)
    pair_total = chosen.shape[0]
    onehot = (chosen[:, None] == jnp.arange(expert_total, dtype=jnp.int32)[None, :]).astype(
        jnp.int32
    )
    ranks = jnp.sum((jnp.cumsum(onehot, axis=0) - onehot) * onehot, axis=1)
    slots = chosen * capacity + ranks
    table = jnp.full((expert_total * capacity,), pair_total, jnp.int32)
    table = table.at[slots].set(jnp.arange(pair_total, dtype=jnp.int32))
    padded = jnp.concatenate([expert_in, jnp.zeros((1, D), jnp.bfloat16)], axis=0)
    outgoing = padded[table // TOP].reshape(expert_total, capacity, D)
    arrived_rows = lax.all_to_all(outgoing, ("sp", "dp"), split_axis=0, concat_axis=0, tiled=True)
    row_block = arrived_rows.reshape(-1, D)
    gate_part = jnp.dot(row_block, specialist_switch_matrix[0], preferred_element_type=jnp.float32)
    up_part = jnp.dot(row_block, specialist_expand_matrix[0], preferred_element_type=jnp.float32)
    hidden_units = (jax.nn.silu(gate_part) * up_part).astype(jnp.bfloat16)
    result = jnp.dot(
        hidden_units, specialist_contract_matrix[0], preferred_element_type=jnp.float32
    )
    returned = lax.all_to_all(
        result.astype(jnp.bfloat16).reshape(arrived_rows.shape),
        ("sp", "dp"),
        split_axis=0,
        concat_axis=0,
        tiled=True,
    )
    flat_back = returned.reshape(expert_total * capacity, D)
    pair_rows = flat_back[slots].reshape(tok_rows, TOP, D)
    weights = dispatcher_logits[0]
    weights = weights / jnp.sum(weights, axis=1, keepdims=True)
    combined = jnp.sum(pair_rows.astype(jnp.float32) * weights[:, :, None], axis=1)
    layer_out = residual.astype(jnp.float32) + rms_scale(combined, specialist_branch_scale)
    return layer_out.astype(jnp.bfloat16)[None]


def solution(mesh):
    return jax.shard_map(
        shards,
        mesh=mesh,
        in_specs=(
            P("dp", "sp", None),
            P("dp", "sp", None),
            P("dp", "sp", None),
            P("dp", "sp", None),
            P("dp", "sp", None),
            P("dp", "sp", None),
            P(),
            P(None, "dp"),
            P(),
            P(),
            P(("sp", "dp"), None, None),
            P(("sp", "dp"), None, None),
            P(("sp", "dp"), None, None),
            P(),
            P("dp", "sp", None),
            P("dp", "sp", None),
        ),
        out_specs=P("dp", "sp", None),
        check_vma=False,
    )
```

profile of v0, /device:TPU:0, one launch (start us, length us, event | category | flops | bytes accessed | tf_op | source)
XLA Modules:
  0.0 359.1 jit_solution(7891554783984080326)
XLA Ops:
  6.5 0.7 all-gather.2.cloned.1.call-update
  7.6 1.0 copy.180
  8.6 7.3 %all-to-all-start.1 = ((bf16[128,16,128]{0,2,1:T(8,128)(2,1)}), bf16[128,16,128]{0,2,1:T(8,128)(2,1)S(1)}, u32[]{:S(2)}, u32[]{:S(2)}) async-start(bf16[128,16,128]{0,2,1:T(8,128)(2,1)} %bitcast.6), calls=%async_computation.1 | async-start | bytes 1048576 | tf_op jit(solution)/shard_map/all_to_all | solution.py:84
  15.9 1.0 copy.185
  16.9 13.4 %all-to-all-done.1 = bf16[128,16,128]{0,2,1:T(8,128)(2,1)S(1)} async-done(((bf16[128,16,128]{0,2,1:T(8,128)(2,1)}), bf16[128,16,128]{0,2,1:T(8,128)(2,1)S(1)}, u32[]{:S(2)}, u32[]{:S(2)}) %all-to-all-start.1) | async-done | bytes 524320 | tf_op jit(solution)/shard_map/all_to_all | solution.py:84
  30.3 3.6 %all-to-all-start.2 = ((bf16[128,16,128]{0,2,1:T(8,128)(2,1)}), bf16[128,16,128]{0,2,1:T(8,128)(2,1)S(1)}, u32[]{:S(2)}, u32[]{:S(2)}) async-start(bf16[128,16,128]{0,2,1:T(8,128)(2,1)} %bitcast.13), calls=%async_computation.2 | async-start | bytes 1048576 | tf_op jit(solution)/shard_map/all_to_all | solution.py:82
  34.0 1.0 copy.177
  35.0 13.7 %all-to-all-done.2 = bf16[128,16,128]{0,2,1:T(8,128)(2,1)S(1)} async-done(((bf16[128,16,128]{0,2,1:T(8,128)(2,1)}), bf16[128,16,128]{0,2,1:T(8,128)(2,1)S(1)}, u32[]{:S(2)}, u32[]{:S(2)}) %all-to-all-start.2) | async-done | bytes 524320 | tf_op jit(solution)/shard_map/all_to_all | solution.py:82
  48.7 4.2 %all-to-all-start = ((bf16[128,16,128]{0,2,1:T(8,128)(2,1)}), bf16[128,16,128]{0,2,1:T(8,128)(2,1)}, u32[]{:S(2)}, u32[]{:S(2)}) async-start(bf16[128,16,128]{0,2,1:T(8,128)(2,1)} %bitcast.1), calls=%async_computation | async-start | bytes 1048576 | tf_op jit(solution)/shard_map/all_to_all | solution.py:81
  52.9 1.3 copy.191
  54.2 0.8 dynamic_slice.3
  56.1 11.0 %all-to-all-done = bf16[128,16,128]{0,2,1:T(8,128)(2,1)} async-done(((bf16[128,16,128]{0,2,1:T(8,128)(2,1)}), bf16[128,16,128]{0,2,1:T(8,128)(2,1)}, u32[]{:S(2)}, u32[]{:S(2)}) %all-to-all-start) | async-done | bytes 524320 | tf_op jit(solution)/shard_map/all_to_all | solution.py:81
  67.1 3.7 %all-to-all-start.3 = ((bf16[128,16,256]{0,2,1:T(8,128)(2,1)}), bf16[128,16,256]{0,2,1:T(8,128)(2,1)S(1)}, u32[]{:S(2)}, u32[]{:S(2)}) async-start(bf16[128,16,256]{0,2,1:T(8,128)(2,1)} %bitcast.18), calls=%async_computation.3 | async-start | bytes 2097152 | tf_op jit(solution)/shard_map/all_to_all | solution.py:83
  71.7 1.2 convert_element_type.100
  72.9 1.3 copy.187
  74.2 1.1 convert_multiply_fusion.2
  75.4 1.3 copy.179
  76.7 4.0 %exponential_multiply_fusion = (f32[16,64,2,128]{3,0,1,2:T(8,128)}, f32[16,64,2,128]{3,0,1,2:T(8,128)S(1)}, f32[16,64,2,128]{3,0,1,2:T(8,128)S(1)}) fusion(f32[16,64,2,128]{3,0,1,2:T(8,128)S(1)} %fusion.30, f32[16,64,2,128]{3,1,0,2:T(8,128)} %bitcast.106, f32[16,2,128]{2,0,1:T(8,128)S(1)} %slice_bitcast_fusion, f32[16,64,2,128]{3,1,0,2:T(8,128)} %bitcast.107), kind=kLoop, calls=%fused_computation.49 | loop fusion | flops 1310720 | bytes 6307840 | tf_op jit(solution)/shard_map/mul | solution.py:41
  80.7 3.5 convolution_select_fusion
  84.2 12.4 %all-to-all-done.3 = bf16[128,16,256]{0,2,1:T(8,128)(2,1)S(1)} async-done(((bf16[128,16,256]{0,2,1:T(8,128)(2,1)}), bf16[128,16,256]{0,2,1:T(8,128)(2,1)S(1)}, u32[]{:S(2)}, u32[]{:S(2)}) %all-to-all-start.3) | async-done | bytes 1048608 | tf_op jit(solution)/shard_map/all_to_all | solution.py:83
  97.1 3.7 %fusion.27 = f32[16,2,128,256]{3,2,1,0:T(8,128)S(1)} fusion(f32[16,64,2,128]{3,0,1,2:T(8,128)} %get-tuple-element.7, bf16[16,64,2,256]{3,1,0,2:T(8,128)(2,1)S(1)} %bitcast.97), kind=kOutput, calls=%fused_computation.40 | convolution fusion | flops 805306368 | bytes 6291456 | tf_op jit(solution)/shard_map/nshk,nshv->nhkv/dot_general | solution.py:42
  101.1 1.6 copy-done
  102.7 0.7 slice.136
  103.7 0.9 copy-done.6
  104.9 0.7 copy-done.8
  105.6 0.8 pad_add_fusion
  106.4 4.2 %pad.30 = f32[4,2,128,256]{3,2,1,0:T(8,128)} pad(f32[2,2,128,256]{3,2,1,0:T(8,128)} %pad_add_fusion, f32[]{:T(128)} %constant.27.clone.1), padding=1_0_1x0_0_0x0_0_0x0_0_0 | pad | bytes 1572868 | tf_op jit(solution)/shard_map/pad | solution.py:44
  110.6 1.1 fusion.57
  111.7 0.8 pad_maximum_fusion.2
  112.6 4.1 %pad.29 = f32[4,2,128,256]{3,2,1,0:T(8,128)} pad(f32[2,2,128,256]{3,2,1,0:T(8,128)} %pad_maximum_fusion.2, f32[]{:T(128)} %constant.27.clone.1), padding=0_1_1x0_0_0x0_0_0x0_0_0 | pad | bytes 1572868 | tf_op jit(solution)/shard_map/pad | solution.py:44
  116.7 2.8 add.160
  119.7 0.7 copy-done.11
  120.4 1.1 pad_maximum_fusion.1
  121.5 3.9 %pad.31 = f32[8,2,128,256]{3,2,1,0:T(8,128)S(1)} pad(f32[4,2,128,256]{3,2,1,0:T(8,128)} %pad_maximum_fusion.1, f32[]{:T(128)} %constant.27.clone.1), padding=0_1_1x0_0_0x0_0_0x0_0_0 | pad | bytes 3145732 | tf_op jit(solution)/shard_map/pad | solution.py:44
  125.4 6.6 %pad.32 = f32[8,2,128,256]{3,2,1,0:T(8,128)} pad(f32[4,2,128,256]{3,2,1,0:T(8,128)} %add.160, f32[]{:T(128)} %constant.27.clone.1), padding=1_0_1x0_0_0x0_0_0x0_0_0 | pad | bytes 3145732 | tf_op jit(solution)/shard_map/pad | solution.py:44
  132.0 3.2 add.162
  135.2 11.5 %pad.66 = f32[16,2,128,256]{3,2,1,0:T(8,128)} pad(f32[8,2,128,256]{3,2,1,0:T(8,128)} %add.162, f32[]{:T(128)} %constant.27.clone.1), padding=1_0_1x0_0_0x0_0_0x0_0_0 | pad | bytes 6291460
  146.6 2.5 fusion.14
  149.1 1.5 pad_maximum_fusion
  150.6 11.5 %pad.44 = f32[15,2,128,256]{3,2,1,0:T(8,128)} pad(f32[8,2,128,256]{3,2,1,0:T(8,128)} %pad_maximum_fusion, f32[]{:T(128)} %constant.27.clone.1), padding=0_0_1x0_0_0x0_0_0x0_0_0 | pad | bytes 6029316 | tf_op jit(solution)/shard_map/slice | solution.py:45
  162.1 1.0 fusion.35
  163.1 1.2 copy-done.1
  164.3 2.9 fusion.16.clone.4
  167.2 2.9 multiply_reduce_fusion.1
  170.7 2.1 copy.206
  172.7 3.6 %all-to-all-start.4 = ((bf16[1024,2,256]{2,1,0:T(2,128)(2,1)}), bf16[1024,2,256]{2,1,0:T(2,128)(2,1)S(1)}, u32[]{:S(2)}, u32[]{:S(2)}) async-start(bf16[1024,2,256]{2,1,0:T(2,128)(2,1)} %copy.206), calls=%async_computation.4 | async-start | bytes 2097152 | tf_op jit(solution)/shard_map/all_to_all | solution.py:101
  178.0 1.4 scatter_custom_fusion
  179.4 22.9 %all-to-all-done.4 = bf16[1024,2,256]{2,1,0:T(2,128)(2,1)S(1)} async-done(((bf16[1024,2,256]{2,1,0:T(2,128)(2,1)}), bf16[1024,2,256]{2,1,0:T(2,128)(2,1)S(1)}, u32[]{:S(2)}, u32[]{:S(2)}) %all-to-all-start.4) | async-done | bytes 1048608 | tf_op jit(solution)/shard_map/all_to_all | solution.py:101
  202.5 0.9 copy.208
  203.5 8.3 %multiply_reduce_fusion.3 = (f32[128]{0:T(128)S(1)}, f32[128,2048]{1,0:T(8,128)S(1)}) fusion(bf16[128,4096]{0,1:T(8,128)(2,1)S(1)} %bitcast.99, bf16[4096,2048]{1,0:T(8,128)(2,1)} %all-gather.2.cloned.1.call-done), kind=kOutput, calls=%fused_computation.47 | convolution fusion | flops 2148532224 | bytes 18874880 | tf_op jit(solution)/shard_map/dot_general | solution.py:103
  212.7 3.2 gather_fusion
  215.9 1.8 reshape.176
  217.6 52.3 %all_to_all.67 = bf16[32,13,2048]{2,1,0:T(8,128)(2,1)} all-to-all(bf16[32,13,2048]{2,1,0:T(8,128)(2,1)S(1)} %reshape.176), channel_id=1, replica_groups=mesh['sp'=8,'dp'=4] {'sp','dp'}, dimensions={0} | all-to-all | bytes 3407872 | tf_op jit(solution)/shard_map/all_to_all | solution.py:128
  269.9 1.8 reshape.177
  271.8 5.3 %fusion.4 = f32[416,1024]{1,0:T(8,128)} fusion(bf16[416,2048]{1,0:T(8,128)(2,1)S(1)} %reshape.177, bf16[1,2048,1024]{2,1,0:T(8,128)(2,1)} %param.26), kind=kOutput, calls=%fused_computation.7 | convolution fusion | flops 1744830464 | bytes 7602176 | tf_op jit(solution)/shard_map/dot_general | solution.py:130
  277.1 8.9 %fusion.8 = bf16[416,2048]{1,0:T(8,128)(2,1)} fusion(bf16[1,1024,2048]{2,1,0:T(8,128)(2,1)} %param.28, f32[416,1024]{1,0:T(8,128)} %fusion.4, bf16[416,2048]{1,0:T(8,128)(2,1)S(1)} %reshape.177, bf16[1,2048,1024]{2,1,0:T(8,128)(2,1)} %param.27), kind=kOutput, calls=%fused_computation.12 | convolution fusion | flops 3493068800 | bytes 13500416 | tf_op jit(solution)/shard_map/dot_general | solution.py:133
  286.0 2.8 reshape.178
  288.8 4.1 %all-to-all-start.6 = ((bf16[32,13,2048]{2,1,0:T(8,128)(2,1)}), bf16[32,13,2048]{2,1,0:T(8,128)(2,1)}, u32[]{:S(2)}, u32[]{:S(2)}) async-start(bf16[32,13,2048]{2,1,0:T(8,128)(2,1)} %reshape.178), calls=%async_computation.6 | async-start | bytes 4194304 | tf_op jit(solution)/shard_map/all_to_all | solution.py:136
  293.1 48.2 %all-to-all-done.6 = bf16[32,13,2048]{2,1,0:T(8,128)(2,1)} async-done(((bf16[32,13,2048]{2,1,0:T(8,128)(2,1)}), bf16[32,13,2048]{2,1,0:T(8,128)(2,1)}, u32[]{:S(2)}, u32[]{:S(2)}) %all-to-all-start.6) | async-done | bytes 1703968 | tf_op jit(solution)/shard_map/all_to_all | solution.py:136
  341.3 1.8 reshape.179
  343.1 2.3 gather_fusion.1
  345.5 2.4 reshape.182
  347.9 3.2 multiply_reduce_fusion
  351.2 1.0 fusion.40
  (107 shorter events, 7.6 us)
Async XLA Ops:
  6.5 1.0 copy-start.12
  6.5 196.9 %all-gather.2.cloned.1.call-start = ((), (), s32[]{:S(2)}) async-start(), calls=%async_computation.7 | async-start | bytes 20971520 | tf_op jit(solution)/shard_map/all_gather | solution.py:105
  7.6 8.3 %copy-start.13 = (bf16[1,128,2048]{2,1,0:T(8,128)(2,1)S(1)}, bf16[1,128,2048]{2,1,0:T(8,128)(2,1)}, u32[]{:S(2)}) copy-start(bf16[1,128,2048]{2,1,0:T(8,128)(2,1)} %param.18) | copy-start | bytes 1572868
  7.6 26.4 %copy-start.14 = (bf16[1,128,2048]{2,1,0:T(8,128)(2,1)S(1)}, bf16[1,128,2048]{2,1,0:T(8,128)(2,1)}, u32[]{:S(2)}) copy-start(bf16[1,128,2048]{2,1,0:T(8,128)(2,1)} %param.17) | copy-start | bytes 1572868
  8.6 21.8 %all-to-all-start.1 = ((bf16[128,16,128]{0,2,1:T(8,128)(2,1)}), bf16[128,16,128]{0,2,1:T(8,128)(2,1)S(1)}, u32[]{:S(2)}, u32[]{:S(2)}) async-start(bf16[128,16,128]{0,2,1:T(8,128)(2,1)} %bitcast.6), calls=%async_computation.1 | async-start | bytes 1048576 | tf_op jit(solution)/shard_map/all_to_all | solution.py:84
  15.9 37.0 %copy-start.19 = (f32[1,2,1024]{2,1,0:T(2,128)S(1)}, f32[1,2,1024]{2,1,0:T(2,128)}, u32[]{:S(2)}) copy-start(f32[1,2,1024]{2,1,0:T(2,128)} %param.21) | copy-start | bytes 24580
  15.9 37.0 %copy-start.10 = (bf16[1,128,4096]{2,1,0:T(8,128)(2,1)S(1)}, bf16[1,128,4096]{2,1,0:T(8,128)(2,1)}, u32[]{:S(2)}) copy-start(bf16[1,128,4096]{2,1,0:T(8,128)(2,1)} %param.19) | copy-start | bytes 3145732
  30.3 18.3 %all-to-all-start.2 = ((bf16[128,16,128]{0,2,1:T(8,128)(2,1)}), bf16[128,16,128]{0,2,1:T(8,128)(2,1)S(1)}, u32[]{:S(2)}, u32[]{:S(2)}) async-start(bf16[128,16,128]{0,2,1:T(8,128)(2,1)} %bitcast.13), calls=%async_computation.2 | async-start | bytes 1048576 | tf_op jit(solution)/shard_map/all_to_all | solution.py:82
  48.7 6.5 %copy-start.9 = (bf16[128,16,128]{0,2,1:T(8,128)(2,1)}, bf16[128,16,128]{0,2,1:T(8,128)(2,1)S(1)}, u32[]{:S(2)}) copy-start(bf16[128,16,128]{0,2,1:T(8,128)(2,1)S(1)} %all-to-all-done.2) | copy-start | bytes 1572868
  48.7 18.4 %all-to-all-start = ((bf16[128,16,128]{0,2,1:T(8,128)(2,1)}), bf16[128,16,128]{0,2,1:T(8,128)(2,1)}, u32[]{:S(2)}, u32[]{:S(2)}) async-start(bf16[128,16,128]{0,2,1:T(8,128)(2,1)} %bitcast.1), calls=%async_computation | async-start | bytes 1048576 | tf_op jit(solution)/shard_map/all_to_all | solution.py:81
  67.1 29.5 %all-to-all-start.3 = ((bf16[128,16,256]{0,2,1:T(8,128)(2,1)}), bf16[128,16,256]{0,2,1:T(8,128)(2,1)S(1)}, u32[]{:S(2)}, u32[]{:S(2)}) async-start(bf16[128,16,256]{0,2,1:T(8,128)(2,1)} %bitcast.18), calls=%async_computation.3 | async-start | bytes 2097152 | tf_op jit(solution)/shard_map/all_to_all | solution.py:83
  97.1 3.7 %copy-start.2 = (bf16[8,128,2,256]{3,1,0,2:T(8,128)(2,1)}, bf16[8,128,2,256]{3,1,0,2:T(8,128)(2,1)S(1)}, u32[]{:S(2)}) copy-start(bf16[8,128,2,256]{3,1,0,2:T(8,128)(2,1)S(1)} %copy.193) | copy-start | bytes 3145732
  100.8 1.9 copy-start
  103.7 1.0 copy-start.6
  104.9 0.7 copy-start.8
  116.7 2.8 copy-start.4
  116.7 2.8 copy-start.5
  119.5 1.0 copy-start.11
  146.6 2.5 slice-start
  150.6 11.5 %copy-start.3 = (bf16[8,128,2,256]{3,1,0,2:T(8,128)(2,1)S(1)}, bf16[8,128,2,256]{3,1,0,2:T(8,128)(2,1)}, u32[]{:S(2)}) copy-start(bf16[8,128,2,256]{3,1,0,2:T(8,128)(2,1)} %copy-done.2) | copy-start | bytes 3145732
  150.6 11.5 %copy-start.7 = (f32[16,2,64,64]{3,2,1,0:T(8,128)S(1)}, f32[16,2,64,64]{3,2,1,0:T(8,128)}, u32[]{:S(2)}) copy-start(f32[16,2,64,64]{3,2,1,0:T(8,128)} %convolution_select_fusion) | copy-start | bytes 1572868
  162.1 2.2 copy-start.1
  170.7 5.7 %copy-start.20 = (s32[1,128,2]{1,2,0:T(2,128)S(1)}, s32[1,128,2]{1,2,0:T(2,128)}, u32[]{:S(2)}) copy-start(s32[1,128,2]{1,2,0:T(2,128)} %param.30) | copy-start | bytes 3076
  172.7 29.6 %all-to-all-start.4 = ((bf16[1024,2,256]{2,1,0:T(2,128)(2,1)}), bf16[1024,2,256]{2,1,0:T(2,128)(2,1)S(1)}, u32[]{:S(2)}, u32[]{:S(2)}) async-start(bf16[1024,2,256]{2,1,0:T(2,128)(2,1)} %copy.206), calls=%async_computation.4 | async-start | bytes 2097152 | tf_op jit(solution)/shard_map/all_to_all | solution.py:101
  203.4 8.3 %copy-start.15 = (bf16[1,128,2048]{2,1,0:T(8,128)(2,1)S(1)}, bf16[1,128,2048]{2,1,0:T(8,128)(2,1)}, u32[]{:S(2)}) copy-start(bf16[1,128,2048]{2,1,0:T(8,128)(2,1)} %param.16) | copy-start | bytes 1572868
  203.5 8.3 %copy-start.16 = (f32[2048]{0:T(1024)S(1)}, f32[2048]{0:T(1024)}, u32[]{:S(2)}) copy-start(f32[2048]{0:T(1024)} %param.24) | copy-start | bytes 24580
  211.7 0.7 copy-start.17
  288.8 4.1 %copy-start.21 = (f32[1,128,2]{1,2,0:T(2,128)S(1)}, f32[1,128,2]{1,2,0:T(2,128)}, u32[]{:S(2)}) copy-start(f32[1,128,2]{1,2,0:T(2,128)} %param.31) | copy-start | bytes 3076
  288.8 52.5 %all-to-all-start.6 = ((bf16[32,13,2048]{2,1,0:T(8,128)(2,1)}), bf16[32,13,2048]{2,1,0:T(8,128)(2,1)}, u32[]{:S(2)}, u32[]{:S(2)}) async-start(bf16[32,13,2048]{2,1,0:T(8,128)(2,1)} %reshape.178), calls=%async_computation.6 | async-start | bytes 4194304 | tf_op jit(solution)/shard_map/all_to_all | solution.py:136
  347.8 3.3 copy-start.18
Sparse Core Ops, SparseCore 0:
  8.9 108.6 all-gather.1
where the time goes:
time: 361 us; the launch traced here: 359 us
  waiting for transfers between devices  122 us (34%)
  local copies, waits for them, and re-layouts  78.8 us (22%)
  blocking collectives  52.3 us (14%)
  matrix products  33.5 us (9%)
  other arithmetic  31.6 us (9%)
  starting transfers between devices  26.5 us (7%)
  between operations  14 us (4%)
    all_to_all x1, blocking collectives, shards(): lax.all_to_all(outgoing, ('sp', 'dp'), split_axis=0, concat_axis=0, tiled...  52.3 us
    all_to_all x1, waiting for transfers between devices, shards(): lax.all_to_all(result.astype(jnp.bfloat16).reshape(arrived_rows.shape), (...  48.2 us
    all_to_all x1, waiting for transfers between devices, shards(): lax.all_to_all(normed, 'sp', split_axis=0, concat_axis=1, tiled=True)  22.9 us
    unnamed x50, local copies, waits for them, and re-layouts  21.6 us
    pad x4, local copies, waits for them, and re-layouts, block_attention(): lax.associative_scan(combine_states, (decays, updates), axis=0)  18.7 us
    all_to_all x1, waiting for transfers between devices, shards(): lax.all_to_all(key_local, 'sp', split_axis=1, concat_axis=0, tiled=True)  13.7 us
    all_to_all x1, waiting for transfers between devices, shards(): lax.all_to_all(decay_local, 'sp', split_axis=1, concat_axis=0, tiled=True)  13.4 us
    all_to_all x1, waiting for transfers between devices, shards(): lax.all_to_all(value_local, 'sp', split_axis=1, concat_axis=0, tiled=True)  12.4 us
  transfers between devices with their start and end apart: 7, of which 6 were waited for; matrix products, arithmetic and copies ran while one was open for 26% of the time, Pallas kernels for 0%

commit v1 on v0

--- a/solution.py
+++ b/solution.py
@@ -12,6 +12,13 @@
 epsilon = 1e-06
 softness_factor = 16.0
 highest = lax.Precision.HIGHEST
+
+
+def trade_parts(array, axis, split, join):
+    count = lax.axis_size(axis)
+    blocks = jnp.stack(jnp.split(array, count, axis=split), axis=0)
+    blocks = lax.all_to_all(blocks, axis, split_axis=0, concat_axis=0)
+    return jnp.concatenate(blocks, axis=join)
 
 
 def rms_scale(values, gain):
@@ -98,7 +105,7 @@
         own_heads, DV
     )
     normed = rms_scale(outputs, gains).astype(jnp.bfloat16)
-    attention_group_result = lax.all_to_all(normed, "sp", split_axis=0, concat_axis=1, tiled=True)
+    attention_group_result = trade_parts(normed, "sp", 0, 1)
     flat_heads = attention_group_result.reshape(tok_rows, ATTENTION_GROUPS * DV)
     projected = jnp.dot(
         flat_heads,

time: 361 us -> 364 us (level)
    unnamed x50 -> x57, local copies, waits for them, and re-layouts: 21.6 us -> 26.2 us
  transfers between devices with their start and end apart: 7 -> 7, of which waited for: 6 -> 6; matrix products, arithmetic and copies ran while one was open for 26% -> 27% of each run, Pallas kernels for 0% -> 0%
where the time goes in v1:
time: 364 us; the launch traced here: 362 us
  waiting for transfers between devices  123 us (34%)
  local copies, waits for them, and re-layouts  81.6 us (22%)
  blocking collectives  52.3 us (14%)
  matrix products  33.5 us (9%)
  other arithmetic  31.6 us (9%)
  starting transfers between devices  26.2 us (7%)
  between operations  14 us (4%)
    all_to_all x1, blocking collectives, shards(): lax.all_to_all(outgoing, ('sp', 'dp'), split_axis=0, concat_axis=0, tiled...  52.3 us
    all_to_all x1, waiting for transfers between devices, shards(): lax.all_to_all(result.astype(jnp.bfloat16).reshape(arrived_rows.shape), (...  48.5 us
    unnamed x57, local copies, waits for them, and re-layouts  26.2 us
    all_to_all x1, waiting for transfers between devices, trade_parts(): blocks = lax.all_to_all(blocks, axis, split_axis=0, concat_axis=0)  22.9 us
    pad x4, local copies, waits for them, and re-layouts, block_attention(): lax.associative_scan(combine_states, (decays, updates), axis=0)  18.7 us
    all_to_all x1, waiting for transfers between devices, shards(): lax.all_to_all(key_local, 'sp', split_axis=1, concat_axis=0, tiled=True)  13.7 us
    all_to_all x1, waiting for transfers between devices, shards(): lax.all_to_all(decay_local, 'sp', split_axis=1, concat_axis=0, tiled=True)  13.4 us
    all_to_all x1, waiting for transfers between devices, shards(): lax.all_to_all(value_local, 'sp', split_axis=1, concat_axis=0, tiled=True)  12.4 us
  transfers between devices with their start and end apart: 7, of which 6 were waited for; matrix products, arithmetic and copies ran while one was open for 27% of the time, Pallas kernels for 0%

profile of v1, /device:TPU:0, one launch (start us, length us, event | category | flops | bytes accessed | tf_op | source)
XLA Modules:
  0.0 361.9 jit_solution(1728737718007709858)
XLA Ops:
  6.5 0.7 all-gather.2.cloned.1.call-update
  7.6 1.0 copy.178
  8.6 7.3 %all-to-all-start.1 = ((bf16[128,16,128]{0,2,1:T(8,128)(2,1)}), bf16[128,16,128]{0,2,1:T(8,128)(2,1)S(1)}, u32[]{:S(2)}, u32[]{:S(2)}) async-start(bf16[128,16,128]{0,2,1:T(8,128)(2,1)} %bitcast.6), calls=%async_computation.1 | async-start | bytes 1048576 | tf_op jit(solution)/shard_map/all_to_all | solution.py:91
  15.9 1.0 copy.183
  16.9 13.4 %all-to-all-done.1 = bf16[128,16,128]{0,2,1:T(8,128)(2,1)S(1)} async-done(((bf16[128,16,128]{0,2,1:T(8,128)(2,1)}), bf16[128,16,128]{0,2,1:T(8,128)(2,1)S(1)}, u32[]{:S(2)}, u32[]{:S(2)}) %all-to-all-start.1) | async-done | bytes 524320 | tf_op jit(solution)/shard_map/all_to_all | solution.py:91
  30.3 3.6 %all-to-all-start.2 = ((bf16[128,16,128]{0,2,1:T(8,128)(2,1)}), bf16[128,16,128]{0,2,1:T(8,128)(2,1)S(1)}, u32[]{:S(2)}, u32[]{:S(2)}) async-start(bf16[128,16,128]{0,2,1:T(8,128)(2,1)} %bitcast.13), calls=%async_computation.2 | async-start | bytes 1048576 | tf_op jit(solution)/shard_map/all_to_all | solution.py:89
  34.0 1.0 copy.175
  35.0 13.7 %all-to-all-done.2 = bf16[128,16,128]{0,2,1:T(8,128)(2,1)S(1)} async-done(((bf16[128,16,128]{0,2,1:T(8,128)(2,1)}), bf16[128,16,128]{0,2,1:T(8,128)(2,1)S(1)}, u32[]{:S(2)}, u32[]{:S(2)}) %all-to-all-start.2) | async-done | bytes 524320 | tf_op jit(solution)/shard_map/all_to_all | solution.py:89
  48.7 4.2 %all-to-all-start = ((bf16[128,16,128]{0,2,1:T(8,128)(2,1)}), bf16[128,16,128]{0,2,1:T(8,128)(2,1)}, u32[]{:S(2)}, u32[]{:S(2)}) async-start(bf16[128,16,128]{0,2,1:T(8,128)(2,1)} %bitcast.1), calls=%async_computation | async-start | bytes 1048576 | tf_op jit(solution)/shard_map/all_to_all | solution.py:88
  52.9 1.3 copy.189
  54.2 0.8 dynamic_slice.3
  56.1 11.0 %all-to-all-done = bf16[128,16,128]{0,2,1:T(8,128)(2,1)} async-done(((bf16[128,16,128]{0,2,1:T(8,128)(2,1)}), bf16[128,16,128]{0,2,1:T(8,128)(2,1)}, u32[]{:S(2)}, u32[]{:S(2)}) %all-to-all-start) | async-done | bytes 524320 | tf_op jit(solution)/shard_map/all_to_all | solution.py:88
  67.1 3.7 %all-to-all-start.3 = ((bf16[128,16,256]{0,2,1:T(8,128)(2,1)}), bf16[128,16,256]{0,2,1:T(8,128)(2,1)S(1)}, u32[]{:S(2)}, u32[]{:S(2)}) async-start(bf16[128,16,256]{0,2,1:T(8,128)(2,1)} %bitcast.18), calls=%async_computation.3 | async-start | bytes 2097152 | tf_op jit(solution)/shard_map/all_to_all | solution.py:90
  71.7 1.2 convert_element_type.100
  72.9 1.3 copy.185
  74.2 1.1 convert_multiply_fusion.2
  75.4 1.3 copy.177
  76.7 4.0 %exponential_multiply_fusion = (f32[16,64,2,128]{3,0,1,2:T(8,128)}, f32[16,64,2,128]{3,0,1,2:T(8,128)S(1)}, f32[16,64,2,128]{3,0,1,2:T(8,128)S(1)}) fusion(f32[16,64,2,128]{3,0,1,2:T(8,128)S(1)} %fusion.30, f32[16,64,2,128]{3,1,0,2:T(8,128)} %bitcast.136, f32[16,2,128]{2,0,1:T(8,128)S(1)} %slice_bitcast_fusion.8, f32[16,64,2,128]{3,1,0,2:T(8,128)} %bitcast.137), kind=kLoop, calls=%fused_computation.49 | loop fusion | flops 1310720 | bytes 6307840 | tf_op jit(solution)/shard_map/mul | solution.py:48
  80.7 3.5 convolution_select_fusion
  84.2 12.4 %all-to-all-done.3 = bf16[128,16,256]{0,2,1:T(8,128)(2,1)S(1)} async-done(((bf16[128,16,256]{0,2,1:T(8,128)(2,1)}), bf16[128,16,256]{0,2,1:T(8,128)(2,1)S(1)}, u32[]{:S(2)}, u32[]{:S(2)}) %all-to-all-start.3) | async-done | bytes 1048608 | tf_op jit(solution)/shard_map/all_to_all | solution.py:90
  97.1 3.7 %fusion.27 = f32[16,2,128,256]{3,2,1,0:T(8,128)S(1)} fusion(f32[16,64,2,128]{3,0,1,2:T(8,128)} %get-tuple-element.7, bf16[16,64,2,256]{3,1,0,2:T(8,128)(2,1)S(1)} %bitcast.127), kind=kOutput, calls=%fused_computation.40 | convolution fusion | flops 805306368 | bytes 6291456 | tf_op jit(solution)/shard_map/nshk,nshv->nhkv/dot_general | solution.py:49
  101.1 1.6 copy-done
  102.7 0.7 slice.136
  103.7 0.9 copy-done.6
  104.9 0.7 copy-done.8
  105.6 0.8 pad_add_fusion
  106.4 4.2 %pad.30 = f32[4,2,128,256]{3,2,1,0:T(8,128)} pad(f32[2,2,128,256]{3,2,1,0:T(8,128)} %pad_add_fusion, f32[]{:T(128)} %constant.27.clone.1), padding=1_0_1x0_0_0x0_0_0x0_0_0 | pad | bytes 1572868 | tf_op jit(solution)/shard_map/pad | solution.py:51
  110.6 1.1 fusion.65
  111.7 0.8 pad_maximum_fusion.2
  112.6 4.1 %pad.29 = f32[4,2,128,256]{3,2,1,0:T(8,128)} pad(f32[2,2,128,256]{3,2,1,0:T(8,128)} %pad_maximum_fusion.2, f32[]{:T(128)} %constant.27.clone.1), padding=0_1_1x0_0_0x0_0_0x0_0_0 | pad | bytes 1572868 | tf_op jit(solution)/shard_map/pad | solution.py:51
  116.7 2.8 add.160
  119.7 0.7 copy-done.11
  120.4 1.1 pad_maximum_fusion.1
  121.5 3.9 %pad.31 = f32[8,2,128,256]{3,2,1,0:T(8,128)S(1)} pad(f32[4,2,128,256]{3,2,1,0:T(8,128)} %pad_maximum_fusion.1, f32[]{:T(128)} %constant.27.clone.1), padding=0_1_1x0_0_0x0_0_0x0_0_0 | pad | bytes 3145732 | tf_op jit(solution)/shard_map/pad | solution.py:51
  125.4 6.6 %pad.32 = f32[8,2,128,256]{3,2,1,0:T(8,128)} pad(f32[4,2,128,256]{3,2,1,0:T(8,128)} %add.160, f32[]{:T(128)} %constant.27.clone.1), padding=1_0_1x0_0_0x0_0_0x0_0_0 | pad | bytes 3145732 | tf_op jit(solution)/shard_map/pad | solution.py:51
  132.0 3.2 add.162
  135.2 11.5 %pad.66 = f32[16,2,128,256]{3,2,1,0:T(8,128)} pad(f32[8,2,128,256]{3,2,1,0:T(8,128)} %add.162, f32[]{:T(128)} %constant.27.clone.1), padding=1_0_1x0_0_0x0_0_0x0_0_0 | pad | bytes 6291460
  146.6 2.5 fusion.14
  149.1 1.5 pad_maximum_fusion
  150.6 11.5 %pad.44 = f32[15,2,128,256]{3,2,1,0:T(8,128)} pad(f32[8,2,128,256]{3,2,1,0:T(8,128)} %pad_maximum_fusion, f32[]{:T(128)} %constant.27.clone.1), padding=0_0_1x0_0_0x0_0_0x0_0_0 | pad | bytes 6029316 | tf_op jit(solution)/shard_map/slice | solution.py:52
  162.1 1.0 fusion.35
  163.1 1.2 copy-done.1
  164.3 2.9 fusion.16.clone.4
  167.2 2.9 multiply_reduce_fusion.1
  171.3 0.7 fusion.50
  174.6 0.7 fusion.45
  175.9 3.6 %all-to-all-start.4 = ((bf16[8,128,2,256]{3,1,2,0:T(8,128)(2,1)}), bf16[8,128,2,256]{3,1,2,0:T(8,128)(2,1)S(1)}, u32[]{:S(2)}, u32[]{:S(2)}) async-start(bf16[8,128,2,256]{3,1,2,0:T(8,128)(2,1)} %fusion.44), calls=%async_computation.4 | async-start | bytes 2097152 | tf_op jit(solution)/shard_map/all_to_all | solution.py:20
  181.2 1.4 scatter_custom_fusion
  182.6 22.9 %all-to-all-done.4 = bf16[8,128,2,256]{3,1,2,0:T(8,128)(2,1)S(1)} async-done(((bf16[8,128,2,256]{3,1,2,0:T(8,128)(2,1)}), bf16[8,128,2,256]{3,1,2,0:T(8,128)(2,1)S(1)}, u32[]{:S(2)}, u32[]{:S(2)}) %all-to-all-start.4) | async-done | bytes 1048608 | tf_op jit(solution)/shard_map/all_to_all | solution.py:20
  206.3 8.3 %multiply_reduce_fusion.3 = (f32[128]{0:T(128)S(1)}, f32[128,2048]{1,0:T(8,128)S(1)}) fusion(bf16[128,4096]{0,1:T(8,128)(2,1)S(1)} %bitcast.129, bf16[4096,2048]{1,0:T(8,128)(2,1)} %all-gather.2.cloned.1.call-done), kind=kOutput, calls=%fused_computation.47 | convolution fusion | flops 2148532224 | bytes 18874880 | tf_op jit(solution)/shard_map/dot_general | solution.py:110
  215.5 3.2 gather_fusion
  218.7 1.8 reshape.175
  220.4 52.3 %all_to_all.57 = bf16[32,13,2048]{2,1,0:T(8,128)(2,1)} all-to-all(bf16[32,13,2048]{2,1,0:T(8,128)(2,1)S(1)} %reshape.175), channel_id=1, replica_groups=mesh['sp'=8,'dp'=4] {'sp','dp'}, dimensions={0} | all-to-all | bytes 3407872 | tf_op jit(solution)/shard_map/all_to_all | solution.py:135
  272.7 1.8 reshape.176
  274.6 5.3 %fusion.4 = f32[416,1024]{1,0:T(8,128)} fusion(bf16[416,2048]{1,0:T(8,128)(2,1)S(1)} %reshape.176, bf16[1,2048,1024]{2,1,0:T(8,128)(2,1)} %param.26), kind=kOutput, calls=%fused_computation.7 | convolution fusion | flops 1744830464 | bytes 7602176 | tf_op jit(solution)/shard_map/dot_general | solution.py:137
  279.9 8.9 %fusion.8 = bf16[416,2048]{1,0:T(8,128)(2,1)} fusion(bf16[1,1024,2048]{2,1,0:T(8,128)(2,1)} %param.28, f32[416,1024]{1,0:T(8,128)} %fusion.4, bf16[416,2048]{1,0:T(8,128)(2,1)S(1)} %reshape.176, bf16[1,2048,1024]{2,1,0:T(8,128)(2,1)} %param.27), kind=kOutput, calls=%fused_computation.12 | convolution fusion | flops 3493068800 | bytes 13500416 | tf_op jit(solution)/shard_map/dot_general | solution.py:140
  288.8 2.8 reshape.177
  291.6 3.8 %all-to-all-start.6 = ((bf16[32,13,2048]{2,1,0:T(8,128)(2,1)}), bf16[32,13,2048]{2,1,0:T(8,128)(2,1)}, u32[]{:S(2)}, u32[]{:S(2)}) async-start(bf16[32,13,2048]{2,1,0:T(8,128)(2,1)} %reshape.177), calls=%async_computation.6 | async-start | bytes 4194304 | tf_op jit(solution)/shard_map/all_to_all | solution.py:143
  295.5 48.5 %all-to-all-done.6 = bf16[32,13,2048]{2,1,0:T(8,128)(2,1)} async-done(((bf16[32,13,2048]{2,1,0:T(8,128)(2,1)}), bf16[32,13,2048]{2,1,0:T(8,128)(2,1)}, u32[]{:S(2)}, u32[]{:S(2)}) %all-to-all-start.6) | async-done | bytes 1703968 | tf_op jit(solution)/shard_map/all_to_all | solution.py:143
  344.1 1.8 reshape.178
  345.9 2.3 gather_fusion.1
  348.3 2.4 reshape.181
  350.6 3.2 multiply_reduce_fusion
  354.0 1.0 fusion.40
  (113 shorter events, 12.0 us)
Async XLA Ops:
  6.5 1.0 copy-start.12
  6.5 199.7 %all-gather.2.cloned.1.call-start = ((), (), s32[]{:S(2)}) async-start(), calls=%async_computation.7 | async-start | bytes 20971520 | tf_op jit(solution)/shard_map/all_gather | solution.py:112
  7.6 8.3 %copy-start.13 = (bf16[1,128,2048]{2,1,0:T(8,128)(2,1)S(1)}, bf16[1,128,2048]{2,1,0:T(8,128)(2,1)}, u32[]{:S(2)}) copy-start(bf16[1,128,2048]{2,1,0:T(8,128)(2,1)} %param.18) | copy-start | bytes 1572868
  7.6 26.4 %copy-start.14 = (bf16[1,128,2048]{2,1,0:T(8,128)(2,1)S(1)}, bf16[1,128,2048]{2,1,0:T(8,128)(2,1)}, u32[]{:S(2)}) copy-start(bf16[1,128,2048]{2,1,0:T(8,128)(2,1)} %param.17) | copy-start | bytes 1572868
  8.6 21.8 %all-to-all-start.1 = ((bf16[128,16,128]{0,2,1:T(8,128)(2,1)}), bf16[128,16,128]{0,2,1:T(8,128)(2,1)S(1)}, u32[]{:S(2)}, u32[]{:S(2)}) async-start(bf16[128,16,128]{0,2,1:T(8,128)(2,1)} %bitcast.6), calls=%async_computation.1 | async-start | bytes 1048576 | tf_op jit(solution)/shard_map/all_to_all | solution.py:91
  15.9 37.0 %copy-start.19 = (f32[1,2,1024]{2,1,0:T(2,128)S(1)}, f32[1,2,1024]{2,1,0:T(2,128)}, u32[]{:S(2)}) copy-start(f32[1,2,1024]{2,1,0:T(2,128)} %param.21) | copy-start | bytes 24580
  15.9 37.0 %copy-start.10 = (bf16[1,128,4096]{2,1,0:T(8,128)(2,1)S(1)}, bf16[1,128,4096]{2,1,0:T(8,128)(2,1)}, u32[]{:S(2)}) copy-start(bf16[1,128,4096]{2,1,0:T(8,128)(2,1)} %param.19) | copy-start | bytes 3145732
  30.3 18.3 %all-to-all-start.2 = ((bf16[128,16,128]{0,2,1:T(8,128)(2,1)}), bf16[128,16,128]{0,2,1:T(8,128)(2,1)S(1)}, u32[]{:S(2)}, u32[]{:S(2)}) async-start(bf16[128,16,128]{0,2,1:T(8,128)(2,1)} %bitcast.13), calls=%async_computation.2 | async-start | bytes 1048576 | tf_op jit(solution)/shard_map/all_to_all | solution.py:89
  48.7 6.5 %copy-start.9 = (bf16[128,16,128]{0,2,1:T(8,128)(2,1)}, bf16[128,16,128]{0,2,1:T(8,128)(2,1)S(1)}, u32[]{:S(2)}) copy-start(bf16[128,16,128]{0,2,1:T(8,128)(2,1)S(1)} %all-to-all-done.2) | copy-start | bytes 1572868
  48.7 18.4 %all-to-all-start = ((bf16[128,16,128]{0,2,1:T(8,128)(2,1)}), bf16[128,16,128]{0,2,1:T(8,128)(2,1)}, u32[]{:S(2)}, u32[]{:S(2)}) async-start(bf16[128,16,128]{0,2,1:T(8,128)(2,1)} %bitcast.1), calls=%async_computation | async-start | bytes 1048576 | tf_op jit(solution)/shard_map/all_to_all | solution.py:88
  67.1 29.5 %all-to-all-start.3 = ((bf16[128,16,256]{0,2,1:T(8,128)(2,1)}), bf16[128,16,256]{0,2,1:T(8,128)(2,1)S(1)}, u32[]{:S(2)}, u32[]{:S(2)}) async-start(bf16[128,16,256]{0,2,1:T(8,128)(2,1)} %bitcast.18), calls=%async_computation.3 | async-start | bytes 2097152 | tf_op jit(solution)/shard_map/all_to_all | solution.py:90
  97.1 3.7 %copy-start.2 = (bf16[8,128,2,256]{3,1,0,2:T(8,128)(2,1)}, bf16[8,128,2,256]{3,1,0,2:T(8,128)(2,1)S(1)}, u32[]{:S(2)}) copy-start(bf16[8,128,2,256]{3,1,0,2:T(8,128)(2,1)S(1)} %copy.191) | copy-start | bytes 3145732
  100.8 1.9 copy-start
  103.7 1.0 copy-start.6
  104.9 0.7 copy-start.8
  116.7 2.8 copy-start.4
  116.7 2.8 copy-start.5
  119.5 1.0 copy-start.11
  146.6 2.5 slice-start
  150.6 11.5 %copy-start.3 = (bf16[8,128,2,256]{3,1,0,2:T(8,128)(2,1)S(1)}, bf16[8,128,2,256]{3,1,0,2:T(8,128)(2,1)}, u32[]{:S(2)}) copy-start(bf16[8,128,2,256]{3,1,0,2:T(8,128)(2,1)} %copy-done.2) | copy-start | bytes 3145732
  150.6 11.5 %copy-start.7 = (f32[16,2,64,64]{3,2,1,0:T(8,128)S(1)}, f32[16,2,64,64]{3,2,1,0:T(8,128)}, u32[]{:S(2)}) copy-start(f32[16,2,64,64]{3,2,1,0:T(8,128)} %convolution_select_fusion) | copy-start | bytes 1572868
  162.1 2.2 copy-start.1
  170.7 8.9 %copy-start.20 = (s32[1,128,2]{1,2,0:T(2,128)S(1)}, s32[1,128,2]{1,2,0:T(2,128)}, u32[]{:S(2)}) copy-start(s32[1,128,2]{1,2,0:T(2,128)} %param.30) | copy-start | bytes 3076
  175.9 29.6 %all-to-all-start.4 = ((bf16[8,128,2,256]{3,1,2,0:T(8,128)(2,1)}), bf16[8,128,2,256]{3,1,2,0:T(8,128)(2,1)S(1)}, u32[]{:S(2)}, u32[]{:S(2)}) async-start(bf16[8,128,2,256]{3,1,2,0:T(8,128)(2,1)} %fusion.44), calls=%async_computation.4 | async-start | bytes 2097152 | tf_op jit(solution)/shard_map/all_to_all | solution.py:20
  206.2 8.3 %copy-start.15 = (bf16[1,128,2048]{2,1,0:T(8,128)(2,1)S(1)}, bf16[1,128,2048]{2,1,0:T(8,128)(2,1)}, u32[]{:S(2)}) copy-start(bf16[1,128,2048]{2,1,0:T(8,128)(2,1)} %param.16) | copy-start | bytes 1572868
  206.2 8.3 %copy-start.16 = (f32[2048]{0:T(1024)S(1)}, f32[2048]{0:T(1024)}, u32[]{:S(2)}) copy-start(f32[2048]{0:T(1024)} %param.24) | copy-start | bytes 24580
  214.5 0.7 copy-start.17
  291.6 3.8 %copy-start.21 = (f32[1,128,2]{1,2,0:T(2,128)S(1)}, f32[1,128,2]{1,2,0:T(2,128)}, u32[]{:S(2)}) copy-start(f32[1,128,2]{1,2,0:T(2,128)} %param.31) | copy-start | bytes 3076
  291.6 52.5 %all-to-all-start.6 = ((bf16[32,13,2048]{2,1,0:T(8,128)(2,1)}), bf16[32,13,2048]{2,1,0:T(8,128)(2,1)}, u32[]{:S(2)}, u32[]{:S(2)}) async-start(bf16[32,13,2048]{2,1,0:T(8,128)(2,1)} %reshape.177), calls=%async_computation.6 | async-start | bytes 4194304 | tf_op jit(solution)/shard_map/all_to_all | solution.py:143
  350.6 3.3 copy-start.18
Sparse Core Ops, SparseCore 0:
  8.9 108.6 all-gather.1
